TPU v7x, 128 devices: a whole 4x4x4 slice. The times are simulated.
128 devices in a mesh: rep: 2 (over z_hi), fs: 32 (over z_lo, y, x), tp: 2 (over core).
Axes of the slice: x: 4, y: 4, z: 4 (z_hi: 2, z_lo: 2; z = z_hi * 2 + z_lo), core: 2. Of those that a mesh axis runs over, the one named last changes fastest.
Arguments:
- tokens: bfloat16 [64, 1024, 2048], P(('rep', 'fs'), 'tp'), may hold values from -6 to 6
- mix_gain: float32 [2048], replicated, may hold values from 0.1 to 1.9
- out_gate_w: float32 [2048, 1024], P('fs', 'tp'), may hold values from -0.125 to 0.125
- in_gate_w: float32 [2048, 1024], P('fs', 'tp'), may hold values from -0.125 to 0.125
- value_w: float32 [2048, 1024], P('fs', 'tp'), may hold values from -0.125 to 0.125
- out_gate_scale: float32 [1024], P(('tp', 'fs')), may hold values from 0.28 to 3.5
- in_gate_scale: float32 [1024], P(('tp', 'fs')), may hold values from 0.5 to 2
- value_scale: float32 [1024], P(('tp', 'fs')), may hold values from 0.5 to 2
- mix_taps: float32 [3, 1024], P(None, 'tp'), may hold values from -3.5 to 3.5
- conv_gain: float32 [1024], P('tp'), may hold values from 0.1 to 1.9
- out_proj_w: float32 [1024, 2048], P('tp', 'fs'), may hold values from -0.1875 to 0.1875
- proj_scale: float32 [2048], P('fs'), may hold values from 0.5 to 2
- ffn_gain: float32 [2048], replicated, may hold values from 0.1 to 1.9
- gate_w: float32 [2048, 2816], P('fs', 'tp'), may hold values from -0.125 to 0.125
- up_w: float32 [2048, 2816], P('fs', 'tp'), may hold values from -0.125 to 0.125
- gate_scale: float32 [2816], P(('tp', 'fs')), may hold values from 0.5 to 2
- up_scale: float32 [2816], P(('tp', 'fs')), may hold values from 0.5 to 2
- gate_taps: float32 [3, 2816], P(None, 'tp'), may hold values from -3.5 to 3.5
- up_taps: float32 [3, 2816], P(None, 'tp'), may hold values from -3.5 to 3.5
- gate_bias: float32 [2816], P('tp'), may hold values from -3 to 3
- up_bias: float32 [2816], P('tp'), may hold values from -3 to 3
- down_w: float32 [2816, 2048], P('tp', 'fs'), may hold values from -0.109375 to 0.109375
- down_scale: float32 [2048], P('fs'), may hold values from 0.5 to 2
Outputs:
- layer_out: bfloat16 [64, 1024, 2048], P(('rep', 'fs'), 'tp')
All inputs are finite; a program needn't handle non-finite values.
Results may differ from a plain program's by a relative error of at most 0.02.
Values may be sent and summed in bfloat16 or wider, within the bound.
A program may use at most 128 MiB of HBM per device.

v0:
```python
import jax
import jax.numpy as jnp
from jax import lax
from jax.sharding import PartitionSpec as P

epsilon = 1e-06


def joined_along(parts, dim):
    shape = list(parts.shape[1:])
    shape[dim] *= parts.shape[0]
    return jnp.moveaxis(parts, 0, dim).reshape(shape)


def gather_packed(arrays, axis, dims):
    ravelled = jnp.concatenate([a.reshape(-1) for a in arrays])
    lines, at, done = (lax.all_gather(ravelled, axis), 0, [])
    for a, dim in zip(arrays, dims):
        parts = lines[:, at : at + a.size].reshape(-1, *a.shape)
        done.append(joined_along(parts, dim))
        at += a.size
    return tuple(done)


def side_by_side(arrays, axis, dim, along):
    widths = [a.shape[along] for a in arrays]
    both = jnp.concatenate(arrays, axis=along)
    filled = lax.all_gather(both, axis, axis=dim, tiled=True)
    return tuple(jnp.split(filled, [sum(widths[:k]) for k in range(1, len(widths))], axis=along))


def from_everyone(shard, axis):
    size = lax.axis_size(axis)
    return lax.all_to_all(
        jnp.broadcast_to(shard[None], (size, *shard.shape)), axis, 0, 0, tiled=True
    )


def of_everyone(shard, axis):
    return from_everyone(shard, axis).sum(axis=0)


def collect(shard, axis, dim):
    return joined_along(from_everyone(shard, axis), dim)


def split_up(shard, dim, size):
    before, after = (shard.shape[:dim], shard.shape[dim + 1 :])
    return jnp.moveaxis(shard.reshape(*before, size, -1, *after), dim, 0)


def summed_on_arrival(shard, axis, dim):
    size = lax.axis_size(axis)
    parts = lax.all_to_all(split_up(shard, dim, size), axis, 0, 0, tiled=True)
    return jnp.sum(parts.astype(jnp.float32), axis=0)


def norm_rows(values, gain):
    return values * lax.rsqrt(jnp.mean(values * values, axis=-1, keepdims=True) + epsilon) * gain


def causal_taps(values, taps):
    kernel = taps.shape[0]
    length = values.shape[0]
    padded = jnp.pad(values, ((kernel - 1, 0), (0, 0)))
    total = jnp.zeros(values.shape, jnp.float32)
    for offset in range(kernel):
        total = total + taps[offset] * padded[offset : offset + length]
    return total


def column_block(left, scale_all, piece):
    return jnp.dot(left, piece, preferred_element_type=jnp.float32) * scale_all


def local(
    tokens,
    mix_gain,
    out_gate_w,
    in_gate_w,
    value_w,
    out_gate_scale,
    in_gate_scale,
    value_scale,
    mix_taps,
    conv_gain,
    out_proj_w,
    proj_scale,
    ffn_gain,
    gate_w,
    up_w,
    gate_scale,
    up_scale,
    gate_taps,
    up_taps,
    gate_bias,
    up_bias,
    down_w,
    down_scale,
):
    resid = tokens[0].astype(jnp.float32)
    normed_in = norm_rows(resid, mix_gain).astype(jnp.bfloat16)
    all_rows = lax.all_gather(normed_in, "tp", axis=0, tiled=True)
    whole_outgate, whole_ingate, whole_value, whole_gate, whole_up, whole_proj, whole_down = (
        gather_packed(
            (
                out_gate_scale,
                in_gate_scale,
                value_scale,
                gate_scale,
                up_scale,
                proj_scale,
                down_scale,
            ),
            "fs",
            (0, 0, 0, 0, 0, 0, 0),
        )
    )
    outgate_rows, ingate_rows, value_rows = side_by_side(
        (
            out_gate_w.astype(jnp.bfloat16),
            in_gate_w.astype(jnp.bfloat16),
            value_w.astype(jnp.bfloat16),
        ),
        "fs",
        0,
        1,
    )
    out_gate = (
        jnp.dot(all_rows, outgate_rows, preferred_element_type=jnp.float32) * whole_outgate
    ).astype(jnp.bfloat16)
    in_gate = (
        jnp.dot(all_rows, ingate_rows, preferred_element_type=jnp.float32) * whole_ingate
    ).astype(jnp.bfloat16)
    value_in = (
        jnp.dot(all_rows, value_rows, preferred_element_type=jnp.float32) * whole_value
    ).astype(jnp.bfloat16)
    mixed_in = in_gate.astype(jnp.float32) * value_in.astype(jnp.float32)
    conv_out = (out_gate.astype(jnp.float32) * causal_taps(mixed_in, mix_taps)).astype(jnp.bfloat16)
    conv_float = conv_out.astype(jnp.float32)
    channels = conv_float.shape[1] * lax.axis_size("tp")
    sumsq = of_everyone(jnp.sum(conv_float * conv_float, axis=1), "tp")
    mixed = (conv_float * lax.rsqrt(sumsq / channels + epsilon)[:, None] * conv_gain).astype(
        jnp.bfloat16
    )
    partial_mix = (lambda piece, start: column_block(mixed, whole_proj, piece))(
        collect(out_proj_w.astype(jnp.bfloat16), "fs", 1), jnp.int32(0)
    )
    summed = summed_on_arrival(partial_mix.astype(jnp.bfloat16), "tp", 0)
    first = (resid + summed).astype(jnp.bfloat16)
    resid_two = first.astype(jnp.float32)
    normed_ffn = norm_rows(resid_two, ffn_gain).astype(jnp.bfloat16)
    ffn_all = lax.all_gather(normed_ffn, "tp", axis=0, tiled=True)
    gate_cast = gate_w.astype(jnp.bfloat16)
    up_cast = up_w.astype(jnp.bfloat16)
    pieces = side_by_side((gate_cast, up_cast), "fs", 0, 1)
    gate_sum = jnp.dot(ffn_all, pieces[0], preferred_element_type=jnp.float32)
    up_sum = jnp.dot(ffn_all, pieces[1], preferred_element_type=jnp.float32)
    gate_pre = (gate_sum * whole_gate).astype(jnp.bfloat16)
    up_pre = (up_sum * whole_up).astype(jnp.bfloat16)
    gate_act = causal_taps(gate_pre.astype(jnp.float32), gate_taps) + gate_bias
    up_act = causal_taps(up_pre.astype(jnp.float32), up_taps) + up_bias
    hidden = (jax.nn.silu(gate_act) * up_act).astype(jnp.bfloat16)
    partial_down = column_block(
        hidden, whole_down, lax.all_gather(down_w.astype(jnp.bfloat16), "fs", axis=1, tiled=True)
    )
    summed_two = summed_on_arrival(partial_down.astype(jnp.bfloat16), "tp", 0)
    return (resid_two + summed_two).astype(jnp.bfloat16)[None]


def solution(mesh):
    placed = (
        P(("rep", "fs"), "tp", None),
        P(),
        P("fs", "tp"),
        P("fs", "tp"),
        P("fs", "tp"),
        P(("tp", "fs")),
        P(("tp", "fs")),
        P(("tp", "fs")),
        P(None, "tp"),
        P("tp"),
        P("tp", "fs"),
        P("fs"),
        P(),
        P("fs", "tp"),
        P("fs", "tp"),
        P(("tp", "fs")),
        P(("tp", "fs")),
        P(None, "tp"),
        P(None, "tp"),
        P("tp"),
        P("tp"),
        P("tp", "fs"),
        P("fs"),
    )
    return jax.shard_map(
        local, mesh=mesh, in_specs=placed, out_specs=P(("rep", "fs"), "tp", None), check_vma=False
    )
```

profile of v0, /device:TPU:1, one launch (start us, length us, event | category | flops | bytes accessed | tf_op | source)
XLA Modules:
  0.0 658.0 jit_solution(3495908413047542810)
XLA Ops:
  6.5 2.1 fusion.11
  8.8 3.5 fusion.13
  12.5 0.7 pad_maximum_fusion.1
  13.2 0.7 dynamic-slice
  15.0 135.7 %all-reduce.3 = f32[8448]{0:T(1024)S(1)} all-reduce(f32[8448]{0:T(1024)S(1)} %dynamic-update-slice), channel_id=2, replica_groups=mesh['rep'=2,'fs'=32,'tp'=2] {'fs'}, use_global_device_ids=true, to_apply=%add.3 | all-reduce | flops 8448 | bytes 67584
  151.2 25.6 %all-gather.9.cloned.1.call-done = bf16[2048,1536]{1,0:T(8,128)(2,1)} async-done(((bf16[64,1536]{1,0:T(8,128)(2,1)}), bf16[2048,1536]{1,0:T(8,128)(2,1)}) %all-gather.9.cloned.1.call-update) | async-done | bytes 6291472 | tf_op jit(solution)/shard_map/all_gather | solution.py:28
  176.8 5.4 multiply_convert_fusion.6
  182.6 2.4 convert_multiply_fusion.4
  185.0 3.1 fusion.32
  188.1 24.5 %all_to_all.21 = f32[2,1,1024]{2,1,0:T(1,128)S(1)} all-to-all(f32[2,1,1024]{2,1,0:T(1,128)S(1)} %broadcast_in_dim.4), channel_id=1, replica_groups=mesh['rep'=2,'fs'=32,'tp'=2] {'tp'}, dimensions={0} | all-to-all | bytes 16384 | tf_op jit(solution)/shard_map/all_to_all | solution.py:34
  212.7 1.6 broadcast_in_dim.5
  214.2 6.8 %all-to-all-start.1 = ((bf16[32,512,64]{1,2,0:T(8,128)(2,1)}), bf16[32,512,64]{1,2,0:T(8,128)(2,1)S(1)}, u32[]{:S(2)}, u32[]{:S(2)}) async-start(bf16[32,512,64]{1,2,0:T(8,128)(2,1)} %broadcast_in_dim.5), calls=%async_computation.1 | async-start | bytes 4194304 | tf_op jit(solution)/shard_map/all_to_all | solution.py:34
  221.2 26.7 %all-to-all-done.1 = bf16[32,512,64]{1,2,0:T(8,128)(2,1)S(1)} async-done(((bf16[32,512,64]{1,2,0:T(8,128)(2,1)}), bf16[32,512,64]{1,2,0:T(8,128)(2,1)S(1)}, u32[]{:S(2)}, u32[]{:S(2)}) %all-to-all-start.1) | async-done | bytes 2097184 | tf_op jit(solution)/shard_map/all_to_all | solution.py:34
  247.9 2.6 multiply_convert_fusion.1
  250.5 8.9 %all_to_all.22 = bf16[2,512,2048]{2,1,0:T(8,128)(2,1)S(1)} all-to-all(bf16[2,512,2048]{2,1,0:T(8,128)(2,1)S(1)} %bitcast.45), channel_id=1, replica_groups=mesh['rep'=2,'fs'=32,'tp'=2] {'tp'}, dimensions={0} | all-to-all | bytes 8388608 | tf_op jit(solution)/shard_map/all_to_all | solution.py:54
  259.4 1.0 convert_reduce_fusion.1
  260.4 0.6 copy-done.2
  261.0 0.7 fusion.16
  261.7 1.3 copy-done
  263.0 2.0 fusion.18
  265.2 0.8 pad_maximum_fusion
  266.1 0.7 convert_element_type.142
  267.2 13.0 %all-gather.11.cloned.1.call-done = bf16[1024,2048]{1,0:T(8,128)(2,1)} async-done(((bf16[512,2048]{1,0:T(8,128)(2,1)}), bf16[1024,2048]{1,0:T(8,128)(2,1)}) %all-gather.11.cloned.1.call-update) | async-done | bytes 4194320 | tf_op jit(solution)/shard_map/all_gather | solution.py:153
  280.3 155.1 %all-gather.13.cloned.1.call-done = bf16[2048,2816]{1,0:T(8,128)(2,1)} async-done(((bf16[64,2816]{1,0:T(8,128)(2,1)}), bf16[2048,2816]{1,0:T(8,128)(2,1)}) %all-gather.13.cloned.1.call-update) | async-done | bytes 11534352 | tf_op jit(solution)/shard_map/all_gather | solution.py:28
  435.4 11.8 %fusion.20 = f32[1024,1408]{1,0:T(8,128)} fusion(bf16[1024,2048]{1,0:T(8,128)(2,1)} %all-gather.11.cloned.1.call-done, bf16[2048,2816]{1,0:T(8,128)(2,1)} %all-gather.13.cloned.1.call-done, f32[1408]{0:T(1024)S(1)} %mul.270), kind=kOutput, calls=%fused_computation.28 | convolution fusion | flops 5909905408 | bytes 15734272 | tf_op jit(solution)/shard_map/dot_general | solution.py:157
  447.2 8.5 %fusion.23 = f32[1024,1408]{1,0:T(8,128)} fusion(bf16[1024,2048]{1,0:T(8,128)(2,1)S(1)} %copy-done.24, bf16[2048,2816]{1,0:T(8,128)(2,1)S(1)} %copy-done.21, f32[1408]{0:T(1024)S(1)} %mul.283), kind=kOutput, calls=%fused_computation.29 | convolution fusion | flops 5909905408 | bytes 15736832 | tf_op jit(solution)/shard_map/dot_general | solution.py:158
  455.7 139.5 %all-gather.15.cloned.1.call-done = bf16[1408,2048]{0,1:T(8,128)(2,1)} async-done(((bf16[1408,64]{0,1:T(8,128)(2,1)}), bf16[1408,2048]{0,1:T(8,128)(2,1)}) %all-gather.15.cloned.1.call-update) | async-done | bytes 5767184 | tf_op jit(solution)/shard_map/all_gather | solution.py:165
  595.2 23.3 %multiply_convert_fusion = bf16[1024,2048]{1,0:T(8,128)(2,1)} fusion(bf16[1408,2048]{0,1:T(8,128)(2,1)} %all-gather.15.cloned.1.call-done, f32[2048]{0:T(1024)S(1)} %mul.294, f32[1024,1408]{1,0:T(8,128)} %fusion.23, f32[1024,1408]{1,0:T(8,128)} %fusion.20, f32[1408]{0:T(1024)S(1)} %copy-done.25, f32[1408]{0:T(1024)S(1)} %get-tuple-element.9, ...), kind=kOutput, calls=%fused_computation.1 | convolution fusion | flops 5935726592 | bytes 21549056 | tf_op jit(solution)/shard_map/dot_general | solution.py:73
  618.5 28.2 %all_to_all.23 = bf16[2,512,2048]{2,1,0:T(8,128)(2,1)S(1)} all-to-all(bf16[2,512,2048]{2,1,0:T(8,128)(2,1)} %bitcast.44), channel_id=1, replica_groups=mesh['rep'=2,'fs'=32,'tp'=2] {'tp'}, dimensions={0} | all-to-all | bytes 8388608 | tf_op jit(solution)/shard_map/all_to_all | solution.py:54
  646.7 1.0 convert_reduce_fusion
  647.7 1.2 copy-done.1
  648.9 2.5 fusion.19
  (93 shorter events, 2.4 us)
Async XLA Ops:
  6.5 5.9 copy-start.6
  6.5 5.9 copy-start.7
  6.5 5.9 copy-start.8
  6.5 144.6 %all-gather.7.cloned.1.call-start = ((), (), s32[]{:S(2)}) async-start(), calls=%async_computation.4 | async-start | bytes 6291456 | tf_op jit(solution)/shard_map/all_gather | solution.py:103
  8.7 4.5 copy-start.28
  8.7 5.9 copy-start.14
  8.7 5.9 copy-start.15
  8.7 5.9 copy-start.16
  8.7 5.9 copy-start.17
  8.7 5.9 copy-start.18
  8.7 5.9 copy-start.19
  8.7 5.9 copy-start.20
  8.8 142.3 %copy-start.9 = (f32[512,64]{0,1:T(8,128)S(1)}, f32[512,64]{0,1:T(8,128)}, u32[]{:S(2)}) copy-start(f32[512,64]{0,1:T(8,128)} %param.33) | copy-start | bytes 393220
  8.8 142.4 %copy-start.13 = (f32[3,512]{1,0:T(4,128)S(1)}, f32[3,512]{1,0:T(4,128)}, u32[]{:S(2)}) copy-start(f32[3,512]{1,0:T(4,128)} %param.31) | copy-start | bytes 18436
  12.4 164.4 %all-gather.9.cloned.1.call-start = ((), (), s32[]{:S(2)}) async-start(), calls=%async_computation.5 | async-start | bytes 6488064 | tf_op jit(solution)/shard_map/all_gather | solution.py:28
  176.8 5.4 copy-start.22
  176.8 5.9 copy-start.23
  188.1 59.8 %copy-start.27 = (f32[512]{0:T(512)S(1)}, f32[512]{0:T(512)}, u32[]{:S(2)}) copy-start(f32[512]{0:T(512)} %param.32) | copy-start | bytes 6148
  214.2 33.7 %all-to-all-start.1 = ((bf16[32,512,64]{1,2,0:T(8,128)(2,1)}), bf16[32,512,64]{1,2,0:T(8,128)(2,1)S(1)}, u32[]{:S(2)}, u32[]{:S(2)}) async-start(bf16[32,512,64]{1,2,0:T(8,128)(2,1)} %broadcast_in_dim.5), calls=%async_computation.1 | async-start | bytes 4194304 | tf_op jit(solution)/shard_map/all_to_all | solution.py:34
  221.0 59.3 %all-gather.11.cloned.1.call-start = ((), (), s32[]{:S(2)}) async-start(), calls=%async_computation.6 | async-start | bytes 6291456 | tf_op jit(solution)/shard_map/all_gather | solution.py:153
  261.0 2.0 copy-start.12
  263.0 2.1 copy-start.3
  263.0 2.2 copy-start.4
  265.1 2.1 copy-start.10
  265.1 2.1 copy-start.11
  265.1 170.3 %all-gather.13.cloned.1.call-start = ((), (), s32[]{:S(2)}) async-start(), calls=%async_computation.7 | async-start | bytes 11894784 | tf_op jit(solution)/shard_map/all_gather | solution.py:28
  266.0 329.2 %all-gather.15.cloned.1.call-start = ((), (), s32[]{:S(2)}) async-start(), calls=%async_computation.8 | async-start | bytes 5947392 | tf_op jit(solution)/shard_map/all_gather | solution.py:165
  435.4 11.8 %copy-start.21 = (bf16[2048,2816]{1,0:T(8,128)(2,1)S(1)}, bf16[2048,2816]{1,0:T(8,128)(2,1)}, u32[]{:S(2)}) copy-start(bf16[2048,2816]{1,0:T(8,128)(2,1)} %all-gather.13.cloned.1.call-done) | copy-start | bytes 34603012
  435.4 11.8 %copy-start.24 = (bf16[1024,2048]{1,0:T(8,128)(2,1)S(1)}, bf16[1024,2048]{1,0:T(8,128)(2,1)}, u32[]{:S(2)}) copy-start(bf16[1024,2048]{1,0:T(8,128)(2,1)} %all-gather.11.cloned.1.call-done) | copy-start | bytes 12582916
  447.2 148.0 %copy-start.25 = (f32[1408]{0:T(1024)S(1)}, f32[1408]{0:T(1024)}, u32[]{:S(2)}) copy-start(f32[1408]{0:T(1024)} %param.43) | copy-start | bytes 16900
  447.2 148.0 %copy-start.26 = (f32[1408]{0:T(1024)S(1)}, f32[1408]{0:T(1024)}, u32[]{:S(2)}) copy-start(f32[1408]{0:T(1024)} %param.42) | copy-start | bytes 16900
  646.7 2.2 copy-start.1
  (3 other events, 4.6 us)
Sparse Core Ops, SparseCore 0:
  12.5 19.9 all-gather.6
  34.1 142.5 all-gather.8
  265.2 15.0 all-gather.10
  281.8 153.5 all-gather.12
  436.9 158.2 all-gather.14
where the time goes:
time: 658 us
  waiting for transfers between devices  360 us (55%)
  blocking collectives  197 us (30%)
  matrix products  57 us (9%)
  other arithmetic  15.1 us (2%)
  between operations  14.3 us (2%)
  local copies, waits for them, and re-layouts  7.36 us (1%)
  starting transfers between devices  6.92 us (1%)
    all_gather x2, waiting for transfers between devices, side_by_side(): filled = lax.all_gather(both, axis, axis=dim, tiled=True)  181 us
    all_gather x1, waiting for transfers between devices, local(): lax.all_gather(down_w.astype(jnp.bfloat16), 'fs', axis=1, tiled=True)  139 us
    unnamed x1, blocking collectives  136 us
    all_to_all x2, blocking collectives, summed_on_arrival(): parts = lax.all_to_all(split_up(shard, dim, size), axis, 0, 0, tiled=True)  37.1 us
    all_to_all x1, waiting for transfers between devices, from_everyone(): lax.all_to_all(jnp.broadcast_to(shard[None], (size, *shard.shape)), axis,...  26.7 us
    dot_general x2, matrix products, column_block(): return jnp.dot(left, piece, preferred_element_type=jnp.float32) * scale_all  25.9 us
    all_to_all x1, blocking collectives, from_everyone(): lax.all_to_all(jnp.broadcast_to(shard[None], (size, *shard.shape)), axis,...  24.5 us
  transfers between devices with their start and end apart: 6, of which 5 were waited for; matrix products, arithmetic and copies ran while one was open for 4% of the time, Pallas kernels for 0%

commit v1 on v0

--- a/solution.py
+++ b/solution.py
@@ -162,7 +162,17 @@
     up_act = causal_taps(up_pre.astype(jnp.float32), up_taps) + up_bias
     hidden = (jax.nn.silu(gate_act) * up_act).astype(jnp.bfloat16)
     partial_down = column_block(
-        hidden, whole_down, lax.all_gather(down_w.astype(jnp.bfloat16), "fs", axis=1, tiled=True)
+        hidden,
+        whole_down,
+        jnp.concatenate(
+            lax.all_to_all(
+                jnp.stack([down_w.astype(jnp.bfloat16)] * lax.axis_size("fs")),
+                concat_axis=0,
+                axis_name="fs",
+                split_axis=0,
+            ),
+            axis=1,
+        ),
     )
     summed_two = summed_on_arrival(partial_down.astype(jnp.bfloat16), "tp", 0)
     return (resid_two + summed_two).astype(jnp.bfloat16)[None]

time: 658 us -> 567 us (0.86)
  waiting for transfers between devices: 360 us -> 264 us
    all_gather x1 -> x0, waiting for transfers between devices: 139 us -> none  [local(): lax.all_gather(down_w.astype(jnp.bfloat16), 'fs', axis=1, tiled=True)]
    all_gather x2, waiting for transfers between devices: 181 us -> 232 us  [side_by_side(): filled = lax.all_gather(both, axis, axis=dim, tiled=True)]
    all_gather x1, waiting for transfers between devices: 13 us -> 5.21 us  [local(): ffn_all = lax.all_gather(normed_ffn, 'tp', axis=0, tiled=True)]
  transfers between devices with their start and end apart: 6 -> 6, of which waited for: 5 -> 4; matrix products, arithmetic and copies ran while one was open for 4% -> 5% of each run, Pallas kernels for 0% -> 0%
where the time goes in v1:
time: 567 us; the launch traced here: 566 us
  waiting for transfers between devices  264 us (47%)
  blocking collectives  194 us (34%)
  matrix products  56.7 us (10%)
  other arithmetic  14.4 us (3%)
  between operations  14.2 us (3%)
  starting transfers between devices  12.4 us (2%)
  local copies, waits for them, and re-layouts  10.5 us (2%)
    all_gather x2, waiting for transfers between devices, side_by_side(): filled = lax.all_gather(both, axis, axis=dim, tiled=True)  232 us
    unnamed x1, blocking collectives  136 us
    all_to_all x2, blocking collectives, summed_on_arrival(): parts = lax.all_to_all(split_up(shard, dim, size), axis, 0, 0, tiled=True)  33.3 us
    all_to_all x1, waiting for transfers between devices, from_everyone(): lax.all_to_all(jnp.broadcast_to(shard[None], (size, *shard.shape)), axis,...  26.7 us
    dot_general x2, matrix products, column_block(): return jnp.dot(left, piece, preferred_element_type=jnp.float32) * scale_all  25.6 us
    all_to_all x1, blocking collectives, from_everyone(): lax.all_to_all(jnp.broadcast_to(shard[None], (size, *shard.shape)), axis,...  24.4 us
    dot_general x1, matrix products, local(): gate_sum = jnp.dot(ffn_all, pieces[0], preferred_element_type=jnp.float32)  11.8 us
  transfers between devices with their start and end apart: 6, of which 4 were waited for; matrix products, arithmetic and copies ran while one was open for 5% of the time, Pallas kernels for 0%

profile of v1, /device:TPU:1, one launch (start us, length us, event | category | flops | bytes accessed | tf_op | source)
XLA Modules:
  0.0 565.9 jit_solution(13670145936547688348)
XLA Ops:
  6.5 2.1 fusion.11
  8.8 3.5 fusion.13
  12.5 0.7 pad_maximum_fusion.1
  13.2 0.6 dynamic-slice
  14.9 136.1 %all-reduce.3 = f32[8448]{0:T(1024)S(1)} all-reduce(f32[8448]{0:T(1024)S(1)} %dynamic-update-slice), channel_id=2, replica_groups=mesh['rep'=2,'fs'=32,'tp'=2] {'fs'}, use_global_device_ids=true, to_apply=%add.3 | all-reduce | flops 8448 | bytes 67584
  151.5 25.2 %all-gather.8.cloned.1.call-done = bf16[2048,1536]{1,0:T(8,128)(2,1)} async-done(((bf16[64,1536]{1,0:T(8,128)(2,1)}), bf16[2048,1536]{1,0:T(8,128)(2,1)}) %all-gather.8.cloned.1.call-update) | async-done | bytes 6291472 | tf_op jit(solution)/shard_map/all_gather | solution.py:28
  176.7 5.4 multiply_convert_fusion.6
  182.5 2.4 convert_multiply_fusion.4
  184.9 3.1 fusion.32
  188.0 24.4 %all_to_all.26 = f32[2,1,1024]{2,1,0:T(1,128)S(1)} all-to-all(f32[2,1,1024]{2,1,0:T(1,128)S(1)} %broadcast_in_dim.4), channel_id=1, replica_groups=mesh['rep'=2,'fs'=32,'tp'=2] {'tp'}, dimensions={0} | all-to-all | bytes 16384 | tf_op jit(solution)/shard_map/all_to_all | solution.py:34
  212.4 1.6 broadcast_in_dim.5
  213.9 7.2 %all-to-all-start.1 = ((bf16[32,512,64]{1,2,0:T(8,128)(2,1)}), bf16[32,512,64]{1,2,0:T(8,128)(2,1)S(1)}, u32[]{:S(2)}, u32[]{:S(2)}) async-start(bf16[32,512,64]{1,2,0:T(8,128)(2,1)} %broadcast_in_dim.5), calls=%async_computation.1 | async-start | bytes 4194304 | tf_op jit(solution)/shard_map/all_to_all | solution.py:34
  221.4 26.7 %all-to-all-done.1 = bf16[32,512,64]{1,2,0:T(8,128)(2,1)S(1)} async-done(((bf16[32,512,64]{1,2,0:T(8,128)(2,1)}), bf16[32,512,64]{1,2,0:T(8,128)(2,1)S(1)}, u32[]{:S(2)}, u32[]{:S(2)}) %all-to-all-start.1) | async-done | bytes 2097184 | tf_op jit(solution)/shard_map/all_to_all | solution.py:34
  248.1 2.6 multiply_convert_fusion.1
  250.7 8.9 %all_to_all.27 = bf16[2,512,2048]{2,1,0:T(8,128)(2,1)S(1)} all-to-all(bf16[2,512,2048]{2,1,0:T(8,128)(2,1)S(1)} %bitcast.48), channel_id=1, replica_groups=mesh['rep'=2,'fs'=32,'tp'=2] {'tp'}, dimensions={0} | all-to-all | bytes 8388608 | tf_op jit(solution)/shard_map/all_to_all | solution.py:54
  259.6 1.0 convert_reduce_fusion.1
  260.6 0.6 copy-done.2
  261.2 0.7 fusion.16
  261.9 1.3 copy-done
  263.1 2.0 fusion.18
  265.3 0.8 pad_maximum_fusion
  266.2 3.2 stack.2
  269.4 5.0 all-to-all-start.3
  274.9 5.2 all-gather.10.cloned.1.call-done
  280.1 206.9 %all-gather.12.cloned.1.call-done = bf16[2048,2816]{1,0:T(8,128)(2,1)} async-done(((bf16[64,2816]{1,0:T(8,128)(2,1)}), bf16[2048,2816]{1,0:T(8,128)(2,1)}) %all-gather.12.cloned.1.call-update) | async-done | bytes 11534352 | tf_op jit(solution)/shard_map/all_gather | solution.py:28
  487.0 11.8 %fusion.20 = f32[1024,1408]{1,0:T(8,128)} fusion(bf16[1024,2048]{1,0:T(8,128)(2,1)} %all-gather.10.cloned.1.call-done, bf16[2048,2816]{1,0:T(8,128)(2,1)} %all-gather.12.cloned.1.call-done, f32[1408]{0:T(1024)S(1)} %mul.270), kind=kOutput, calls=%fused_computation.28 | convolution fusion | flops 5909905408 | bytes 15734272 | tf_op jit(solution)/shard_map/dot_general | solution.py:157
  498.8 8.5 %fusion.23 = f32[1024,1408]{1,0:T(8,128)} fusion(bf16[1024,2048]{1,0:T(8,128)(2,1)S(1)} %copy-done.24, bf16[2048,2816]{1,0:T(8,128)(2,1)S(1)} %copy-done.21, f32[1408]{0:T(1024)S(1)} %mul.283), kind=kOutput, calls=%fused_computation.29 | convolution fusion | flops 5909905408 | bytes 15736832 | tf_op jit(solution)/shard_map/dot_general | solution.py:158
  507.3 23.0 %multiply_convert_fusion = bf16[1024,2048]{1,0:T(8,128)(2,1)} fusion(bf16[1408,2048]{0,1:T(8,128)(2,1)} %bitcast.10, f32[2048]{0:T(1024)S(1)} %mul.294, f32[1024,1408]{1,0:T(8,128)} %fusion.23, f32[1024,1408]{1,0:T(8,128)} %fusion.20, f32[1408]{0:T(1024)S(1)} %copy-done.25, f32[1408]{0:T(1024)S(1)} %get-tuple-element.9, f32[1408]{0:T(1024)S(1)} %get-tuple-element.10, ...), kind=kOutput, calls=%fused_computation.1 | convolution fusion | flops 5935726592 | bytes 21549056 | tf_op jit(solution)/shard_map/dot_general | solution.py:73
  530.3 24.4 %all_to_all.28 = bf16[2,512,2048]{2,1,0:T(8,128)(2,1)S(1)} all-to-all(bf16[2,512,2048]{2,1,0:T(8,128)(2,1)} %bitcast.47), channel_id=1, replica_groups=mesh['rep'=2,'fs'=32,'tp'=2] {'tp'}, dimensions={0} | all-to-all | bytes 8388608 | tf_op jit(solution)/shard_map/all_to_all | solution.py:54
  554.7 1.0 convert_reduce_fusion
  555.6 1.2 copy-done.1
  556.8 2.5 fusion.19
  (93 shorter events, 2.4 us)
Async XLA Ops:
  6.5 5.9 %copy-start.6 = (f32[64,512]{1,0:T(8,128)S(1)}, f32[64,512]{1,0:T(8,128)}, u32[]{:S(2)}) copy-start(f32[64,512]{1,0:T(8,128)} %param.25) | copy-start | bytes 393220
  6.5 5.9 %copy-start.7 = (f32[64,512]{1,0:T(8,128)S(1)}, f32[64,512]{1,0:T(8,128)}, u32[]{:S(2)}) copy-start(f32[64,512]{1,0:T(8,128)} %param.26) | copy-start | bytes 393220
  6.5 5.9 %copy-start.8 = (f32[64,512]{1,0:T(8,128)S(1)}, f32[64,512]{1,0:T(8,128)}, u32[]{:S(2)}) copy-start(f32[64,512]{1,0:T(8,128)} %param.27) | copy-start | bytes 393220
  6.5 144.9 %all-gather.6.cloned.1.call-start = ((), (), s32[]{:S(2)}) async-start(), calls=%async_computation.5 | async-start | bytes 6291456 | tf_op jit(solution)/shard_map/all_gather | solution.py:103
  8.7 4.5 copy-start.28
  8.7 5.8 %copy-start.14 = (f32[16]{0:T(128)S(1)}, f32[16]{0:T(128)}, u32[]{:S(2)}) copy-start(f32[16]{0:T(128)} %param.28) | copy-start | bytes 196
  8.7 5.8 %copy-start.15 = (f32[16]{0:T(128)S(1)}, f32[16]{0:T(128)}, u32[]{:S(2)}) copy-start(f32[16]{0:T(128)} %param.29) | copy-start | bytes 196
  8.7 5.8 %copy-start.16 = (f32[16]{0:T(128)S(1)}, f32[16]{0:T(128)}, u32[]{:S(2)}) copy-start(f32[16]{0:T(128)} %param.30) | copy-start | bytes 196
  8.7 5.8 %copy-start.17 = (f32[44]{0:T(128)S(1)}, f32[44]{0:T(128)}, u32[]{:S(2)}) copy-start(f32[44]{0:T(128)} %param.38) | copy-start | bytes 532
  8.7 5.8 %copy-start.18 = (f32[44]{0:T(128)S(1)}, f32[44]{0:T(128)}, u32[]{:S(2)}) copy-start(f32[44]{0:T(128)} %param.39) | copy-start | bytes 532
  8.7 5.8 %copy-start.19 = (f32[64]{0:T(128)S(1)}, f32[64]{0:T(128)}, u32[]{:S(2)}) copy-start(f32[64]{0:T(128)} %param.34) | copy-start | bytes 772
  8.7 5.8 %copy-start.20 = (f32[64]{0:T(128)S(1)}, f32[64]{0:T(128)}, u32[]{:S(2)}) copy-start(f32[64]{0:T(128)} %param.45) | copy-start | bytes 772
  8.8 142.6 %copy-start.9 = (f32[512,64]{0,1:T(8,128)S(1)}, f32[512,64]{0,1:T(8,128)}, u32[]{:S(2)}) copy-start(f32[512,64]{0,1:T(8,128)} %param.33) | copy-start | bytes 393220
  8.8 142.7 %copy-start.13 = (f32[3,512]{1,0:T(4,128)S(1)}, f32[3,512]{1,0:T(4,128)}, u32[]{:S(2)}) copy-start(f32[3,512]{1,0:T(4,128)} %param.31) | copy-start | bytes 18436
  12.4 164.3 %all-gather.8.cloned.1.call-start = ((), (), s32[]{:S(2)}) async-start(), calls=%async_computation.6 | async-start | bytes 6488064 | tf_op jit(solution)/shard_map/all_gather | solution.py:28
  176.6 5.4 copy-start.22
  176.6 5.9 %copy-start.23 = (bf16[1024,2048]{1,0:T(8,128)(2,1)S(1)}, bf16[1024,2048]{1,0:T(8,128)(2,1)}, u32[]{:S(2)}) copy-start(bf16[1024,2048]{1,0:T(8,128)(2,1)} %all-gather.6.cloned.1.call-done) | copy-start | bytes 12582916
  188.0 60.1 %copy-start.27 = (f32[512]{0:T(512)S(1)}, f32[512]{0:T(512)}, u32[]{:S(2)}) copy-start(f32[512]{0:T(512)} %param.32) | copy-start | bytes 6148
  213.9 34.1 %all-to-all-start.1 = ((bf16[32,512,64]{1,2,0:T(8,128)(2,1)}), bf16[32,512,64]{1,2,0:T(8,128)(2,1)S(1)}, u32[]{:S(2)}, u32[]{:S(2)}) async-start(bf16[32,512,64]{1,2,0:T(8,128)(2,1)} %broadcast_in_dim.5), calls=%async_computation.1 | async-start | bytes 4194304 | tf_op jit(solution)/shard_map/all_to_all | solution.py:34
  221.1 59.0 %all-gather.10.cloned.1.call-start = ((), (), s32[]{:S(2)}) async-start(), calls=%async_computation.7 | async-start | bytes 6291456 | tf_op jit(solution)/shard_map/all_gather | solution.py:153
  261.2 2.0 copy-start.12
  263.1 2.1 copy-start.3
  263.1 2.1 copy-start.4
  265.2 221.8 %all-gather.12.cloned.1.call-start = ((), (), s32[]{:S(2)}) async-start(), calls=%async_computation.8 | async-start | bytes 11894784 | tf_op jit(solution)/shard_map/all_gather | solution.py:28
  269.4 5.4 copy-start.10
  269.4 5.4 copy-start.11
  269.4 237.9 %all-to-all-start.3 = ((bf16[32,1408,64]{1,2,0:T(8,128)(2,1)}), bf16[32,1408,64]{1,2,0:T(8,128)(2,1)}, u32[]{:S(2)}, u32[]{:S(2)}) async-start(bf16[32,1408,64]{1,2,0:T(8,128)(2,1)} %stack.2), calls=%async_computation.3 | async-start | bytes 11534336 | tf_op jit(solution)/shard_map/all_to_all | solution.py:168
  487.0 11.8 %copy-start.21 = (bf16[2048,2816]{1,0:T(8,128)(2,1)S(1)}, bf16[2048,2816]{1,0:T(8,128)(2,1)}, u32[]{:S(2)}) copy-start(bf16[2048,2816]{1,0:T(8,128)(2,1)} %all-gather.12.cloned.1.call-done) | copy-start | bytes 34603012
  487.0 11.8 %copy-start.24 = (bf16[1024,2048]{1,0:T(8,128)(2,1)S(1)}, bf16[1024,2048]{1,0:T(8,128)(2,1)}, u32[]{:S(2)}) copy-start(bf16[1024,2048]{1,0:T(8,128)(2,1)} %all-gather.10.cloned.1.call-done) | copy-start | bytes 12582916
  498.8 8.5 %copy-start.25 = (f32[1408]{0:T(1024)S(1)}, f32[1408]{0:T(1024)}, u32[]{:S(2)}) copy-start(f32[1408]{0:T(1024)} %param.43) | copy-start | bytes 16900
  498.8 8.5 %copy-start.26 = (f32[1408]{0:T(1024)S(1)}, f32[1408]{0:T(1024)}, u32[]{:S(2)}) copy-start(f32[1408]{0:T(1024)} %param.42) | copy-start | bytes 16900
  554.6 2.2 copy-start.1
  (3 other events, 4.5 us)
Sparse Core Ops, SparseCore 0:
  12.5 19.9 all-gather.5
  34.1 142.4 all-gather.7
  265.3 14.7 all-gather.9
  281.6 205.3 all-gather.11
